TPU v7x, 32 devices: a whole 2x2x4 slice. The times are simulated.
32 devices in a mesh: kv: 8 (over z, x), tp: 4 (over y, core).
Axes of the slice: x: 2, y: 2, z: 4, core: 2. Of those that a mesh axis runs over, the one named last changes fastest.
Arguments:
- tokens: bfloat16 [64, 12, 4096], P(None, None, 'kv'), may hold values from -6 to 6
- parents: int32 [64, 12], P('kv'), may hold values from -1 to 10, as said below
- accepted: int32 [64], P('kv'), may hold values from 0 to 6
- state: float32 [64, 64, 64, 128], P('kv', 'tp'), may hold values from -4 to 4
- conv_x: bfloat16 [64, 3, 4096], P('kv', None, 'tp'), may hold values from -6 to 6
- conv_b: bfloat16 [64, 3, 2048], P('kv', None, 'tp'), may hold values from -6 to 6
- conv_c: bfloat16 [64, 3, 2048], P('kv', None, 'tp'), may hold values from -6 to 6
- path_x: bfloat16 [64, 6, 4096], P('kv', None, 'tp'), may hold values from -6 to 6
- path_b: bfloat16 [64, 6, 2048], P('kv', None, 'tp'), may hold values from -6 to 6
- path_c: bfloat16 [64, 6, 2048], P('kv', None, 'tp'), may hold values from -6 to 6
- path_dt: bfloat16 [64, 6, 64], P('kv', None, 'tp'), may hold values from -6 to 6
- gain_in: float32 [4096], replicated, may hold values from 0.1 to 1.9
- w_x: bfloat16 [4096, 4096], P('kv', 'tp'), may hold values from -0.09375 to 0.09375
- w_z: bfloat16 [4096, 4096], P('kv', 'tp'), may hold values from -0.09375 to 0.09375
- w_b: bfloat16 [4096, 2048], P('kv', 'tp'), may hold values from -0.09375 to 0.09375
- w_c: bfloat16 [4096, 2048], P('kv', 'tp'), may hold values from -0.09375 to 0.09375
- w_dt: bfloat16 [4096, 64], replicated, may hold values from -0.09375 to 0.09375
- dt_bias: float32 [64], P('tp'), may hold values from -2 to 1
- a_log: float32 [64], P('tp'), may hold values from -3 to 1.5
- d_skip: float32 [64], P('tp'), may hold values from 0.5 to 1.5
- conv_wx: bfloat16 [4, 4096], P(None, 'tp'), may hold values from -3 to 3
- conv_wb: bfloat16 [4, 2048], P(None, 'tp'), may hold values from -3 to 3
- conv_wc: bfloat16 [4, 2048], P(None, 'tp'), may hold values from -3 to 3
- gain_out: float32 [4096], P('tp'), may hold values from 0.1 to 1.9
- w_out: bfloat16 [4096, 4096], P('tp', 'kv'), may hold values from -0.09375 to 0.09375
Outputs:
- mixed: bfloat16 [64, 12, 4096], P('kv', None, 'tp')
- new_state: float32 [64, 64, 64, 128], P('kv', 'tp')
Inputs may be any that keep to these rules, and one draw needn't show every extreme that they name: `parents`: each proposal's parent is -1 or an earlier proposal of the same sequence; the first proposal's parent is -1.
All inputs are finite; a program needn't handle non-finite values.
Results may differ from a plain program's by a relative error of at most 0.03.
Values may be sent and summed in bfloat16 or wider, within the bound.
A program may use at most 128 MiB of HBM per device.

v0:
```python
import jax
import jax.numpy as jnp
from jax import lax
from jax.sharding import PartitionSpec as P

HPG = 4
EPS = 1e-06
HIGH = lax.Precision.HIGHEST


def conv_window(history, taps, amount):
    values = history.astype(jnp.float32)
    weights = taps.astype(jnp.float32)
    summed = weights[0] * values[:, 0:amount, :]
    for distance in range(1, weights.shape[0]):
        summed = summed + weights[distance] * values[:, distance : distance + amount, :]
    return jax.nn.silu(summed)


def commit_rows(history, accepted, keep):
    picked = accepted[:, None] + jnp.arange(keep, dtype=jnp.int32)[None, :]
    select = (
        picked[:, :, None] == jnp.arange(history.shape[1], dtype=jnp.int32)[None, None, :]
    ).astype(jnp.float32)
    return jnp.einsum("skl,slc->skc", select, history.astype(jnp.float32), precision=HIGH).astype(
        jnp.bfloat16
    )


def replay_state(
    state, history_x, history_b, path_dt, conv_wx, conv_wb, accepted, rate_bias, a_rate, per_group
):
    seq_count, heads, head_dim, state_dim = state.shape
    path_len = path_dt.shape[1]
    path_xs = conv_window(history_x, conv_wx, path_len).reshape(
        seq_count, path_len, heads, head_dim
    )
    path_bs = conv_window(history_b, conv_wb, path_len).reshape(
        seq_count, path_len, heads // per_group, state_dim
    )
    path_bh = jnp.repeat(path_bs, per_group, axis=2)
    path_step = jax.nn.softplus(path_dt.astype(jnp.float32) + rate_bias)
    is_live = (jnp.arange(path_len, dtype=jnp.int32)[None, :] < accepted[:, None]).astype(
        jnp.float32
    )[:, :, None]
    log_decay = path_step * a_rate * is_live
    overall = jnp.sum(log_decay, axis=1)
    tail_sum = overall[:, None, :] - jnp.cumsum(log_decay, axis=1)
    weights = is_live * jnp.exp(tail_sum) * path_step
    grown = jnp.einsum("sjh,sjhp,sjhn->shpn", weights, path_xs, path_bh, precision=HIGH)
    return jnp.exp(overall)[:, :, None, None] * state + grown


def tree_links(parents, keep):
    seq_count, prop_count = parents.shape
    front = jnp.broadcast_to(jnp.arange(-1, keep - 1, dtype=jnp.int32)[None, :], (seq_count, keep))
    parent_ids = jnp.concatenate([front, parents + keep], axis=1)
    nodes = keep + prop_count
    links = (parent_ids[:, :, None] == jnp.arange(nodes, dtype=jnp.int32)[None, None, :]).astype(
        jnp.float32
    )
    identity = jnp.eye(prop_count, dtype=jnp.float32)[None, :, :]
    ancestry = identity + links[:, keep:, keep:]
    for turn in range(prop_count.bit_length()):
        ancestry = jnp.minimum(jnp.einsum("sij,sjk->sik", ancestry, ancestry, precision=HIGH), 1.0)
    return (links, ancestry)


def tree_conv(buffer, rows, taps, links, keep):
    values = jnp.concatenate([buffer, rows], axis=1).astype(jnp.float32)
    weights = taps.astype(jnp.float32)
    last_tap = weights.shape[0] - 1
    summed = weights[last_tap] * values
    reached = values
    for distance in range(1, last_tap + 1):
        reached = jnp.einsum("sij,sjc->sic", links, reached, precision=HIGH)
        summed = summed + weights[last_tap - distance] * reached
    return jax.nn.silu(summed[:, keep:, :])


def tree_mix(
    state,
    post_x,
    post_b,
    post_c,
    rate_rows,
    z_rows,
    ancestry,
    rate_bias,
    a_rate,
    d_skip,
    gain_out,
    per_group,
):
    seq_count, prop_count, _ = post_x.shape
    heads, head_dim, state_dim = (state.shape[1], state.shape[2], state.shape[3])
    groups = heads // per_group
    x_heads = post_x.reshape(seq_count, prop_count, heads, head_dim)
    b_groups = post_b.reshape(seq_count, prop_count, groups, state_dim)
    c_groups = post_c.reshape(seq_count, prop_count, groups, state_dim)
    step_size = jax.nn.softplus(rate_rows.astype(jnp.float32) + rate_bias)
    path_decay = jnp.einsum("sij,sjh->sih", ancestry, step_size * a_rate, precision=HIGH)
    c_heads = jnp.repeat(c_groups, per_group, axis=2)
    carried = (
        jnp.einsum("sihn,shpn->sihp", c_heads, state, precision=HIGH)
        * jnp.exp(path_decay)[:, :, :, None]
    )
    scores = jnp.einsum("sign,sjgn->sgij", c_groups, b_groups, precision=HIGH)
    scores = jnp.repeat(scores, per_group, axis=1)
    decay_t = jnp.transpose(path_decay, (0, 2, 1))
    decay_gap = decay_t[:, :, :, None] - decay_t[:, :, None, :]
    is_live = ancestry[:, None, :, :] > 0.5
    mixing = jnp.where(is_live, jnp.exp(jnp.where(is_live, decay_gap, 0.0)), 0.0)
    mixing = mixing * jnp.transpose(step_size, (0, 2, 1))[:, :, None, :]
    within = jnp.einsum("shij,sjhp->sihp", scores * mixing, x_heads, precision=HIGH)
    heads_out = carried + within + d_skip[None, None, :, None] * x_heads
    heads_out = heads_out.reshape(seq_count, prop_count, heads * head_dim) * jax.nn.silu(
        z_rows.astype(jnp.float32)
    )
    grouped = heads_out.reshape(seq_count, prop_count, groups, per_group * head_dim)
    grouped = grouped * lax.rsqrt(jnp.mean(grouped * grouped, axis=-1, keepdims=True) + EPS)
    return (grouped.reshape(seq_count, prop_count, heads * head_dim) * gain_out).astype(
        jnp.bfloat16
    )


def shards(
    tokens,
    parents,
    accepted,
    state,
    conv_x,
    conv_b,
    conv_c,
    path_x,
    path_b,
    path_c,
    path_dt,
    gain_in,
    w_x,
    w_z,
    w_b,
    w_c,
    w_dt,
    dt_bias,
    a_log,
    d_skip,
    conv_wx,
    conv_wb,
    conv_wc,
    gain_out,
    w_out,
):
    seq_local = state.shape[0]
    proposals = parents.shape[1]
    heads_local = dt_bias.shape[0]
    inner_local = w_x.shape[1]
    group_cols = w_b.shape[1]
    width = gain_in.shape[0]
    keep = conv_wx.shape[0] - 1
    tp_index = lax.axis_index("tp")
    kv_index = lax.axis_index("kv")
    slab_width = tokens.shape[2]
    flat_rows = tokens.reshape(-1, slab_width).astype(jnp.float32)
    gain_part = lax.dynamic_slice_in_dim(gain_in, kv_index * slab_width, slab_width)
    scaled = (flat_rows * gain_part).astype(jnp.bfloat16)
    w_joined = jnp.concatenate([w_x, w_z, w_b, w_c], axis=1)
    joined = lax.psum_scatter(
        jnp.dot(scaled, w_joined, preferred_element_type=jnp.float32).astype(jnp.bfloat16),
        "kv",
        scatter_dimension=0,
        tiled=True,
    ).astype(jnp.float32)
    w_rate = lax.dynamic_slice(
        w_dt, (kv_index * slab_width, tp_index * heads_local), (slab_width, heads_local)
    )
    rate_term = jnp.dot(scaled, w_rate, preferred_element_type=jnp.float32)
    squares = jnp.sum(flat_rows * flat_rows, axis=1)
    rate_raw, squares = (
        lax.psum_scatter(
            rate_term.astype(jnp.bfloat16), "kv", scatter_dimension=0, tiled=True
        ).astype(jnp.float32),
        lax.psum_scatter(
            squares.astype(jnp.bfloat16), "kv", scatter_dimension=0, tiled=True
        ).astype(jnp.float32),
    )
    row_scale = lax.rsqrt(squares / width + EPS)[:, None]

    def column_part(lower, upper):
        return (
            (joined[:, lower:upper] * row_scale)
            .astype(jnp.bfloat16)
            .reshape(seq_local, proposals, upper - lower)
        )

    x_rows = column_part(0, inner_local)
    z_rows = column_part(inner_local, 2 * inner_local)
    b_rows = column_part(2 * inner_local, 2 * inner_local + group_cols)
    c_rows = column_part(2 * inner_local + group_cols, 2 * inner_local + 2 * group_cols)
    rate_rows = (
        (rate_raw * row_scale).astype(jnp.bfloat16).reshape(seq_local, proposals, heads_local)
    )
    a_rate = -jnp.exp(a_log)
    history_x = jnp.concatenate([conv_x, path_x], axis=1)
    history_b = jnp.concatenate([conv_b, path_b], axis=1)
    history_c = jnp.concatenate([conv_c, path_c], axis=1)
    new_state = replay_state(
        state, history_x, history_b, path_dt, conv_wx, conv_wb, accepted, dt_bias, a_rate, HPG
    )
    links, ancestry = tree_links(parents, keep)
    post_x = tree_conv(commit_rows(history_x, accepted, keep), x_rows, conv_wx, links, keep)
    post_b = tree_conv(commit_rows(history_b, accepted, keep), b_rows, conv_wb, links, keep)
    post_c = tree_conv(commit_rows(history_c, accepted, keep), c_rows, conv_wc, links, keep)
    gated = tree_mix(
        new_state,
        post_x,
        post_b,
        post_c,
        rate_rows,
        z_rows,
        ancestry,
        dt_bias,
        a_rate,
        d_skip,
        gain_out,
        HPG,
    )
    gated_flat = gated.reshape(-1, inner_local)
    partial_out = jnp.dot(
        gated_flat,
        lax.all_gather(w_out, "kv", axis=1, tiled=True),
        preferred_element_type=jnp.float32,
    )
    summed = lax.psum_scatter(
        partial_out.astype(jnp.bfloat16), "tp", scatter_dimension=1, tiled=True
    )
    mixed = summed.reshape(seq_local, proposals, -1)
    return (mixed, new_state)


def solution(mesh):
    return jax.shard_map(
        shards,
        mesh=mesh,
        in_specs=(
            P(None, None, "kv"),
            P("kv", None),
            P("kv"),
            P("kv", "tp", None, None),
            P("kv", None, "tp"),
            P("kv", None, "tp"),
            P("kv", None, "tp"),
            P("kv", None, "tp"),
            P("kv", None, "tp"),
            P("kv", None, "tp"),
            P("kv", None, "tp"),
            P(),
            P("kv", "tp"),
            P("kv", "tp"),
            P("kv", "tp"),
            P("kv", "tp"),
            P(),
            P("tp"),
            P("tp"),
            P("tp"),
            P(None, "tp"),
            P(None, "tp"),
            P(None, "tp"),
            P("tp"),
            P("tp", "kv"),
        ),
        out_specs=(P("kv", None, "tp"), P("kv", "tp", None, None)),
        check_vma=False,
    )
```

profile of v0, /device:TPU:0, one launch (start us, length us, event | category | flops | bytes accessed | tf_op | source)
XLA Modules:
  0.0 339.4 jit_solution(18268738023173111490)
XLA Ops:
  7.2 1.7 copy.118
  8.9 1.3 reshape.169
  10.3 0.8 dynamic_slice.6
  11.0 1.7 convolution_convert_fusion.2
  12.7 0.8 copy.153
  13.6 7.0 %convolution_convert_fusion = bf16[768,3072]{1,0:T(8,128)(2,1)} fusion(bf16[512,512]{1,0:T(8,128)(2,1)S(1)} %copy-done.19, bf16[512,512]{1,0:T(8,128)(2,1)} %param.39, bf16[512,1024]{1,0:T(8,128)(2,1)} %param.38, bf16[512,1024]{1,0:T(8,128)(2,1)} %param.37, f32[768,512]{1,0:T(8,128)} %reshape.169, f32[512]{0:T(512)S(1)} %dynamic_slice.6), kind=kOutput, calls=%fused_computation | convolution fusion | flops 2431647744 | bytes 9439232 | tf_op jit(solution)/shard_map/dot_general | solution.py:169
  20.9 0.7 all-gather.2.cloned.1.call-update
  24.4 0.6 dynamic-slice
  25.6 23.1 %all-reduce = bf16[768]{0:T(1024)(128)(2,1)S(1)} all-reduce(bf16[768]{0:T(1024)(128)(2,1)S(1)} %convert_element_type.147), channel_id=3, replica_groups=mesh['kv'=8,'tp'=4] {'kv'}, use_global_device_ids=true, to_apply=%region_4.5.clone | all-reduce | flops 768 | bytes 3072
  50.2 10.3 %multiply_add_fusion = f32[8,16,64,128]{3,2,1,0:T(8,128)} fusion(f32[8,16,64,128]{3,2,1,0:T(8,128)} %param.28, f32[8,6,16,128]{3,1,2,0:T(8,128)S(1)} %bitcast.70, f32[8,16]{1,0:T(8,128)S(1)} %exp.57, f32[8,6,16,64]{3,2,0,1:T(8,128)S(1)} %broadcast_multiply_fusion), kind=kOutput, calls=%fused_computation.2 | convolution fusion | flops 77594624 | bytes 8978944 | tf_op jit(solution)/shard_map/sjh,sjhp,sjhn->shpn/dot_general | solution.py:50
  60.5 18.1 %reduce-scatter.10.cloned.1.call-done = bf16[96,16]{1,0:T(8,128)(2,1)} async-done(((bf16[768,16]{1,0:T(8,128)(2,1)}), bf16[96,16]{1,0:T(8,128)(2,1)}) %reduce-scatter.10.cloned.1.call-update) | async-done | bytes 3088
  78.6 0.8 copy.154
  80.2 96.8 %reduce-scatter.6.cloned.1.call-done = bf16[96,3072]{1,0:T(8,128)(2,1)} async-done(((bf16[768,3072]{1,0:T(8,128)(2,1)}), bf16[96,3072]{1,0:T(8,128)(2,1)}) %reduce-scatter.6.cloned.1.call-update) | async-done | bytes 589840 | tf_op jit(solution)/shard_map/reduce_scatter | solution.py:168
  177.0 1.2 convert_element_type.144
  178.7 0.3 fusion.71
  179.0 0.3 fusion.70
  179.8 0.3 fusion.75
  180.1 0.3 fusion.74
  180.5 1.4 multiply_bitcast_fusion
  181.9 0.8 copy.125
  183.4 0.4 fusion.73
  183.9 0.4 fusion.72
  184.4 0.7 divide_multiply_fusion
  185.5 1.8 fusion.33
  187.5 1.9 fusion.10
  189.5 6.8 %fusion.116 = f32[8,16,64,12]{2,3,1,0:T(8,128)S(1)} fusion(f32[8,16,64,128]{3,2,1,0:T(8,128)S(1)} %copy-done.1, f32[8,12,16,128]{3,1,2,0:T(8,128)S(1)} %bitcast.68), kind=kOutput, calls=%fused_computation.191 | convolution fusion | flops 150994944 | bytes 5373952 | tf_op jit(solution)/shard_map/sihn,shpn->sihp/dot_general | solution.py:105
  196.3 1.1 multiply_reduce_fusion.1
  198.2 105.5 %all-gather.2.cloned.1.call-done = bf16[1024,4096]{1,0:T(8,128)(2,1)} async-done(((bf16[1024,512]{1,0:T(8,128)(2,1)}), bf16[1024,4096]{1,0:T(8,128)(2,1)}) %all-gather.2.cloned.1.call-update) | async-done | bytes 8388624 | tf_op jit(solution)/shard_map/all_gather | solution.py:231
  303.7 5.8 %convolution_convert_fusion.1 = bf16[96,4096]{1,0:T(8,128)(2,1)} fusion(bf16[1024,4096]{1,0:T(8,128)(2,1)} %all-gather.2.cloned.1.call-done, f32[96,1024]{1,0:T(8,128)S(1)} %bitcast.69, f32[96,1024]{1,0:T(8,128)S(1)} %reshape.167, f32[96,1024]{1,0:T(8,128)S(1)} %get-tuple-element.15, f32[1024]{0:T(1024)S(1)} %copy-done.6), kind=kOutput, calls=%fused_computation.1 | convolution fusion | flops 806486016 | bytes 10358784 | tf_op jit(solution)/shard_map/dot_general | solution.py:229
  309.5 21.6 %reduce-scatter.8.cloned.1.call-done = bf16[96,1024]{1,0:T(8,128)(2,1)} async-done(((bf16[96,4096]{1,0:T(8,128)(2,1)}), bf16[96,1024]{1,0:T(8,128)(2,1)}) %reduce-scatter.8.cloned.1.call-update) | async-done | bytes 196624 | tf_op jit(solution)/shard_map/reduce_scatter | solution.py:234
  331.1 1.0 reshape.168
  332.1 0.8 copy.152
  (137 shorter events, 7.9 us)
Async XLA Ops:
  7.2 3.9 %copy-start = (bf16[4096,64]{0,1:T(8,128)(2,1)S(1)}, bf16[4096,64]{0,1:T(8,128)(2,1)}, u32[]{:S(2)}) copy-start(bf16[4096,64]{0,1:T(8,128)(2,1)} %param.41) | copy-start | bytes 1572868
  7.2 71.5 %reduce-scatter.10.cloned.1.call-start = ((), (), s32[]{:S(2)}) async-start(), calls=%async_computation.6 | async-start | bytes 221184
  7.2 6.4 %copy-start.19 = (bf16[512,512]{1,0:T(8,128)(2,1)S(1)}, bf16[512,512]{1,0:T(8,128)(2,1)}, u32[]{:S(2)}) copy-start(bf16[512,512]{1,0:T(8,128)(2,1)} %param.40) | copy-start | bytes 1572868
  13.6 163.4 %reduce-scatter.6.cloned.1.call-start = ((), (), s32[]{:S(2)}) async-start(), calls=%async_computation.3 | async-start | bytes 5308416 | tf_op jit(solution)/shard_map/reduce_scatter | solution.py:168
  20.6 1.1 copy-start.2
  20.6 1.6 copy-start.7
  20.6 1.6 copy-start.11
  20.6 1.7 copy-start.17
  20.7 2.0 copy-start.8
  20.7 2.0 copy-start.12
  20.7 2.3 copy-start.5
  20.7 2.3 copy-start.9
  20.7 2.5 copy-start.10
  20.7 3.0 copy-start.13
  20.8 3.2 copy-start.20
  20.8 3.2 copy-start.4
  20.8 3.2 copy-start.15
  20.8 3.6 %copy-start.21 = (u32[32]{0:T(128)S(1)}, u32[32]{0:T(128)}, u32[]{:S(2)}) copy-start(u32[32]{0:T(128)} %constant.57) | copy-start | bytes 388
  20.8 28.1 %copy-start.16 = (s32[8,12]{1,0:T(8,128)S(1)}, s32[8,12]{1,0:T(8,128)}, u32[]{:S(2)}) copy-start(s32[8,12]{1,0:T(8,128)} %param.26) | copy-start | bytes 1156
  20.8 28.1 %copy-start.14 = (bf16[4,512]{1,0:T(4,128)(2,1)S(1)}, bf16[4,512]{1,0:T(4,128)(2,1)}, u32[]{:S(2)}) copy-start(bf16[4,512]{1,0:T(4,128)(2,1)} %param.47) | copy-start | bytes 12292
  20.8 282.9 %all-gather.2.cloned.1.call-start = ((), (), s32[]{:S(2)}) async-start(), calls=%async_computation.4 | async-start | bytes 9437184 | tf_op jit(solution)/shard_map/all_gather | solution.py:231
  21.6 309.5 %reduce-scatter.8.cloned.1.call-start = ((), (), s32[]{:S(2)}) async-start(), calls=%async_computation.5 | async-start | bytes 983040 | tf_op jit(solution)/shard_map/reduce_scatter | solution.py:234
  185.3 4.1 %copy-start.3 = (f32[8,12,4,128]{3,1,2,0:T(8,128)S(1)}, f32[8,12,4,128]{3,1,2,0:T(8,128)}, u32[]{:S(2)}) copy-start(f32[8,12,4,128]{3,1,2,0:T(8,128)} %copy.125) | copy-start | bytes 589828
  185.5 4.0 %copy-start.1 = (f32[8,16,64,128]{3,2,1,0:T(8,128)S(1)}, f32[8,16,64,128]{3,2,1,0:T(8,128)}, u32[]{:S(2)}) copy-start(f32[8,16,64,128]{3,2,1,0:T(8,128)} %multiply_add_fusion) | copy-start | bytes 12582916
  189.4 6.9 %copy-start.18 = (f32[16]{0:T(128)S(1)}, f32[16]{0:T(128)}, u32[]{:S(2)}) copy-start(f32[16]{0:T(128)} %param.44) | copy-start | bytes 196
  196.3 107.4 %copy-start.6 = (f32[1024]{0:T(1024)S(1)}, f32[1024]{0:T(1024)}, u32[]{:S(2)}) copy-start(f32[1024]{0:T(1024)} %param.48) | copy-start | bytes 12292
Sparse Core Ops, SparseCore 0:
  13.7 64.8 reduce-scatter.9
  82.3 94.7 reduce-scatter.5
  179.1 124.5 all-gather.1
  309.7 21.3 reduce-scatter.7
where the time goes:
time: 340 us; the launch traced here: 339 us
  waiting for transfers between devices  243 us (71%)
  matrix products  39.9 us (12%)
  blocking collectives  23.1 us (7%)
  between operations  15.3 us (4%)
  local copies, waits for them, and re-layouts  12.2 us (4%)
  other arithmetic  6.04 us (2%)
    all_gather x1, waiting for transfers between devices, shards(): lax.all_gather(w_out, 'kv', axis=1, tiled=True)  105 us
    reduce_scatter x1, waiting for transfers between devices, shards(): lax.psum_scatter(jnp.dot(scaled, w_joined, preferred_element_type=jnp.flo...  96.8 us
    unnamed x1, blocking collectives  23.1 us
    reduce_scatter x1, waiting for transfers between devices, shards(): lax.psum_scatter(partial_out.astype(jnp.bfloat16), 'tp', scatter_dimensio...  21.6 us
    unnamed x5, waiting for transfers between devices  18.9 us
    dot_general x1, matrix products, replay_state(): jnp.einsum('sjh,sjhp,sjhn->shpn', weights, path_xs, path_bh, precision=HIGH)  10.3 us
    dot_general x1, matrix products, shards(): jnp.dot(scaled, w_joined, preferred_element_type=jnp.float32)  6.99 us
    dot_general x1, matrix products, tree_mix(): jnp.einsum('sihn,shpn->sihp', c_heads, state, precision=HIGH)  6.82 us
  transfers between devices with their start and end apart: 4, of which 4 were waited for; matrix products, arithmetic and copies ran while one was open for 13% of the time, Pallas kernels for 0%

commit v1 on v0

--- a/solution.py
+++ b/solution.py
@@ -228,7 +228,9 @@
     gated_flat = gated.reshape(-1, inner_local)
     partial_out = jnp.dot(
         gated_flat,
-        lax.all_gather(w_out, "kv", axis=1, tiled=True),
+        jnp.concatenate(
+            lax.all_to_all(jnp.stack([w_out] * lax.axis_size("kv")), "kv", 0, 0), axis=1
+        ),
         preferred_element_type=jnp.float32,
     )
     summed = lax.psum_scatter(

time: 340 us -> 366 us (1.076)
  blocking collectives: 23.1 us -> 149 us
  waiting for transfers between devices: 243 us -> 129 us
  starting transfers between devices: 0.16 us -> 7.53 us
  local copies, waits for them, and re-layouts: 12.2 us -> 17.7 us
    unnamed x1, blocking collectives: 23.1 us -> 149 us
    all_gather x1 -> x0, waiting for transfers between devices: 105 us -> none  [shards(): lax.all_gather(w_out, 'kv', axis=1, tiled=True)]
    unnamed x5 -> x4, waiting for transfers between devices: 18.9 us -> 7.86 us
    all_to_all x0 -> x1, starting transfers between devices: none -> 7.41 us  [shards(): lax.all_to_all(jnp.stack([w_out] * lax.axis_size('kv')), 'kv', 0, 0)]
    another operation x0 -> x1, local copies, waits for them, and re-layouts: none -> 4.31 us  [shards(): jnp.stack([w_out] * lax.axis_size('kv'))]
  transfers between devices with their start and end apart: 4 -> 4, of which waited for: 4 -> 3; matrix products, arithmetic and copies ran while one was open for 13% -> 13% of each run, Pallas kernels for 0% -> 0%
where the time goes in v1:
time: 366 us; the launch traced here: 365 us
  blocking collectives  149 us (41%)
  waiting for transfers between devices  129 us (35%)
  matrix products  40 us (11%)
  local copies, waits for them, and re-layouts  17.7 us (5%)
  between operations  15.4 us (4%)
  starting transfers between devices  7.53 us (2%)
  other arithmetic  5.94 us (2%)
    unnamed x1, blocking collectives  149 us
    reduce_scatter x1, waiting for transfers between devices, shards(): lax.psum_scatter(jnp.dot(scaled, w_joined, preferred_element_type=jnp.flo...  98.2 us
    reduce_scatter x1, waiting for transfers between devices, shards(): lax.psum_scatter(partial_out.astype(jnp.bfloat16), 'tp', scatter_dimensio...  23 us
    dot_general x1, matrix products, replay_state(): jnp.einsum('sjh,sjhp,sjhn->shpn', weights, path_xs, path_bh, precision=HIGH)  10.3 us
    unnamed x4, waiting for transfers between devices  7.86 us
    all_to_all x1, starting transfers between devices, shards(): lax.all_to_all(jnp.stack([w_out] * lax.axis_size('kv')), 'kv', 0, 0)  7.41 us
  transfers between devices with their start and end apart: 4, of which 3 were waited for; matrix products, arithmetic and copies ran while one was open for 13% of the time, Pallas kernels for 0%

profile of v1, /device:TPU:0, one launch (start us, length us, event | category | flops | bytes accessed | tf_op | source)
XLA Modules:
  0.0 365.1 jit_solution(323920717597913856)
XLA Ops:
  7.2 1.5 copy.154
  8.7 4.3 %stack.2 = bf16[8,1024,512]{1,2,0:T(8,128)(2,1)} broadcast(bf16[1024,512]{0,1:T(8,128)(2,1)S(1)} %copy.154), dimensions={1,2} | broadcast | bytes 9437184 | tf_op jit(solution)/shard_map/stack | solution.py:232
  13.0 7.4 %all-to-all-start = ((bf16[8,1024,512]{1,2,0:T(8,128)(2,1)}), bf16[8,1024,512]{1,2,0:T(8,128)(2,1)}, u32[]{:S(2)}, u32[]{:S(2)}) async-start(bf16[8,1024,512]{1,2,0:T(8,128)(2,1)} %stack.2), calls=%async_computation.1 | async-start | bytes 16777216 | tf_op jit(solution)/shard_map/all_to_all | solution.py:232
  20.5 0.5 copy.120
  21.0 1.3 reshape.179
  22.3 0.8 dynamic_slice.6
  23.1 1.7 convolution_convert_fusion.2
  24.8 0.8 copy.156
  25.7 7.1 %convolution_convert_fusion = bf16[768,3072]{1,0:T(8,128)(2,1)} fusion(bf16[512,512]{1,0:T(8,128)(2,1)} %param.40, bf16[512,512]{1,0:T(8,128)(2,1)} %param.39, bf16[512,1024]{1,0:T(8,128)(2,1)} %param.38, bf16[512,1024]{1,0:T(8,128)(2,1)} %param.37, f32[768,512]{1,0:T(8,128)} %reshape.179, f32[512]{0:T(512)S(1)} %dynamic_slice.6), kind=kOutput, calls=%fused_computation | convolution fusion | flops 2431647744 | bytes 9439232 | tf_op jit(solution)/shard_map/dot_general | solution.py:169
  35.8 0.6 dynamic-slice
  37.1 149.4 %all-reduce = bf16[768]{0:T(1024)(128)(2,1)S(1)} all-reduce(bf16[768]{0:T(1024)(128)(2,1)S(1)} %convert_element_type.147), channel_id=3, replica_groups=mesh['kv'=8,'tp'=4] {'kv'}, use_global_device_ids=true, to_apply=%region_4.5.clone | all-reduce | flops 768 | bytes 3072
  186.7 0.6 fusion.113
  188.5 10.3 %multiply_add_fusion = f32[8,16,64,128]{3,2,1,0:T(8,128)} fusion(f32[8,16,64,128]{3,2,1,0:T(8,128)} %param.28, f32[8,6,16,128]{3,1,2,0:T(8,128)S(1)} %bitcast.72, f32[8,16]{1,0:T(8,128)S(1)} %exp.57, f32[8,6,16,64]{3,2,0,1:T(8,128)S(1)} %broadcast_multiply_fusion), kind=kOutput, calls=%fused_computation.2 | convolution fusion | flops 77594624 | bytes 8978944 | tf_op jit(solution)/shard_map/sjh,sjhp,sjhn->shpn/dot_general | solution.py:50
  198.8 7.8 %reduce-scatter.10.cloned.1.call-done = bf16[96,16]{1,0:T(8,128)(2,1)} async-done(((bf16[768,16]{1,0:T(8,128)(2,1)}), bf16[96,16]{1,0:T(8,128)(2,1)}) %reduce-scatter.10.cloned.1.call-update) | async-done | bytes 3088
  206.6 0.8 copy.157
  208.2 98.2 %reduce-scatter.6.cloned.1.call-done = bf16[96,3072]{1,0:T(8,128)(2,1)} async-done(((bf16[768,3072]{1,0:T(8,128)(2,1)}), bf16[96,3072]{1,0:T(8,128)(2,1)}) %reduce-scatter.6.cloned.1.call-update) | async-done | bytes 589840 | tf_op jit(solution)/shard_map/reduce_scatter | solution.py:168
  306.4 1.2 convert_element_type.144
  307.7 1.1 reshape.181
  309.3 0.4 fusion.73
  309.8 0.4 fusion.72
  310.3 0.7 divide_multiply_fusion
  311.3 0.7 fusion.48
  313.4 0.3 fusion.75
  314.2 0.8 multiply_bitcast_fusion
  315.1 0.7 fusion.33
  315.9 1.9 fusion.10
  317.9 6.8 %fusion.116 = f32[8,16,64,12]{2,3,1,0:T(8,128)S(1)} fusion(f32[8,16,64,128]{3,2,1,0:T(8,128)S(1)} %copy-done.1, f32[8,12,16,128]{3,1,2,0:T(8,128)S(1)} %bitcast.71), kind=kOutput, calls=%fused_computation.191 | convolution fusion | flops 150994944 | bytes 5373952 | tf_op jit(solution)/shard_map/sihn,shpn->sihp/dot_general | solution.py:105
  324.8 1.1 multiply_reduce_fusion.1
  326.7 7.0 %convolution_convert_fusion.1 = bf16[96,4096]{1,0:T(8,128)(2,1)} fusion(bf16[1024,4096]{0,1:T(8,128)(2,1)} %bitcast.24, f32[96,1024]{1,0:T(8,128)S(1)} %bitcast.73, f32[96,1024]{1,0:T(8,128)S(1)} %reshape.175, f32[96,1024]{1,0:T(8,128)S(1)} %get-tuple-element.15, f32[1024]{0:T(1024)S(1)} %copy-done.22), kind=kOutput, calls=%fused_computation.1 | convolution fusion | flops 806486016 | bytes 10358784 | tf_op jit(solution)/shard_map/dot_general | solution.py:229
  333.7 23.0 %reduce-scatter.8.cloned.1.call-done = bf16[96,1024]{1,0:T(8,128)(2,1)} async-done(((bf16[96,4096]{1,0:T(8,128)(2,1)}), bf16[96,1024]{1,0:T(8,128)(2,1)}) %reduce-scatter.8.cloned.1.call-update) | async-done | bytes 196624 | tf_op jit(solution)/shard_map/reduce_scatter | solution.py:236
  356.8 1.0 reshape.178
  357.7 0.8 copy.155
  (150 shorter events, 8.7 us)
Async XLA Ops:
  7.2 15.9 %copy-start = (bf16[4096,64]{0,1:T(8,128)(2,1)S(1)}, bf16[4096,64]{0,1:T(8,128)(2,1)}, u32[]{:S(2)}) copy-start(bf16[4096,64]{0,1:T(8,128)(2,1)} %param.41) | copy-start | bytes 1572868
  13.0 7.5 %copy-start.3 = (bf16[64,12,512]{2,0,1:T(8,128)(2,1)S(1)}, bf16[64,12,512]{2,0,1:T(8,128)(2,1)}, u32[]{:S(2)}) copy-start(bf16[64,12,512]{2,0,1:T(8,128)(2,1)} %param.25) | copy-start | bytes 2359300
  13.0 313.6 %all-to-all-start = ((bf16[8,1024,512]{1,2,0:T(8,128)(2,1)}), bf16[8,1024,512]{1,2,0:T(8,128)(2,1)}, u32[]{:S(2)}, u32[]{:S(2)}) async-start(bf16[8,1024,512]{1,2,0:T(8,128)(2,1)} %stack.2), calls=%async_computation.1 | async-start | bytes 16777216 | tf_op jit(solution)/shard_map/all_to_all | solution.py:232
  20.5 186.2 %reduce-scatter.10.cloned.1.call-start = ((), (), s32[]{:S(2)}) async-start(), calls=%async_computation.6 | async-start | bytes 221184
  25.6 280.7 %reduce-scatter.6.cloned.1.call-start = ((), (), s32[]{:S(2)}) async-start(), calls=%async_computation.4 | async-start | bytes 5308416 | tf_op jit(solution)/shard_map/reduce_scatter | solution.py:168
  32.8 0.9 copy-start.5
  32.8 1.0 copy-start.6
  32.8 1.0 copy-start.24
  32.8 1.4 copy-start.7
  32.8 1.4 copy-start.10
  32.8 1.7 copy-start.8
  32.8 1.7 copy-start.11
  32.8 2.0 copy-start.14
  32.9 2.3 copy-start.26
  32.9 2.3 copy-start.4
  32.9 2.3 copy-start.16
  32.9 2.5 copy-start.9
  32.9 2.9 copy-start.27
  32.9 153.6 %copy-start.23 = (s32[8,12]{1,0:T(8,128)S(1)}, s32[8,12]{1,0:T(8,128)}, u32[]{:S(2)}) copy-start(s32[8,12]{1,0:T(8,128)} %param.26) | copy-start | bytes 1156
  32.9 153.7 %copy-start.15 = (bf16[4,512]{1,0:T(4,128)(2,1)S(1)}, bf16[4,512]{1,0:T(4,128)(2,1)}, u32[]{:S(2)}) copy-start(bf16[4,512]{1,0:T(4,128)(2,1)} %param.47) | copy-start | bytes 12292
  33.0 323.8 %reduce-scatter.8.cloned.1.call-start = ((), (), s32[]{:S(2)}) async-start(), calls=%async_computation.5 | async-start | bytes 983040 | tf_op jit(solution)/shard_map/reduce_scatter | solution.py:236
  34.9 153.1 %copy-start.12 = (f32[1,512]{1,0:T(1,128)}, f32[1,512]{1,0:T(1,128)S(1)}, u32[]{:S(2)}) copy-start(f32[1,512]{1,0:T(1,128)S(1)} %get-tuple-element.29) | copy-start | bytes 6148
  186.6 121.0 %copy-start.21 = (f32[96]{0:T(128)}, f32[96]{0:T(128)S(1)}, u32[]{:S(2)}) copy-start(f32[96]{0:T(128)S(1)} %fusion.103) | copy-start | bytes 1156
  311.2 2.9 copy-start.13
  311.2 2.9 copy-start.17
  311.2 2.9 copy-start.18
  311.3 2.9 copy-start.19
  311.3 2.9 copy-start.20
  314.2 3.7 %copy-start.1 = (f32[8,16,64,128]{3,2,1,0:T(8,128)S(1)}, f32[8,16,64,128]{3,2,1,0:T(8,128)}, u32[]{:S(2)}) copy-start(f32[8,16,64,128]{3,2,1,0:T(8,128)} %multiply_add_fusion) | copy-start | bytes 12582916
  317.8 6.9 %copy-start.2 = (f32[8,12,16,64]{3,2,1,0:T(8,128)S(1)}, f32[8,12,16,64]{3,2,1,0:T(8,128)}, u32[]{:S(2)}) copy-start(f32[8,12,16,64]{3,2,1,0:T(8,128)} %reshape.181) | copy-start | bytes 1179652
  317.8 6.9 %copy-start.25 = (f32[16]{0:T(128)S(1)}, f32[16]{0:T(128)}, u32[]{:S(2)}) copy-start(f32[16]{0:T(128)} %param.44) | copy-start | bytes 196
  324.8 1.9 copy-start.22
Sparse Core Ops, SparseCore 0:
  25.8 180.8 reduce-scatter.9
  210.3 96.0 reduce-scatter.5
  333.9 22.8 reduce-scatter.7
